TPU v7x, 512 devices: a 8x2x16 block of a 8x8x16 slice. The times are simulated.
512 devices in a mesh: grp: 2 (over y), fs: 32 (over z, core), tp: 8 (over x).
Axes of the slice: x: 8, y: 2, z: 16, core: 2. Of those that a mesh axis runs over, the one named last changes fastest.
The devices are a block of a 8x8x16 slice.
Arguments:
- tokens: bfloat16 [24576, 2048], P(('grp', 'fs'), 'tp'), parts along dimension 0, may hold values from -6 to 6
- norm_gain: float32 [2048], P('fs'), may hold values from 0.1 to 1.9
- gate_weight: float32 [32, 2048, 1024], P(None, 'fs', 'tp'), may hold values from -0.125 to 0.125
- up_weight: float32 [32, 2048, 1024], P(None, 'fs', 'tp'), may hold values from -0.125 to 0.125
- down_weight: float32 [32, 1024, 2048], P(None, 'fs', 'tp'), may hold values from -0.1875 to 0.1875
- routes: int32 [24576, 2], P(('grp', 'fs')), parts along dimension 0, may hold values from 0 to 31, as said below
- route_weights: float32 [24576, 2], P(('grp', 'fs')), parts along dimension 0, may hold values from 0.2 to 1
Outputs:
- gate_serve: bfloat16 [64, 2048, 1024], P(('grp', 'fs'), None, 'tp'), parts along dimension 0
- up_serve: bfloat16 [64, 2048, 1024], P(('grp', 'fs'), None, 'tp'), parts along dimension 0
- down_serve: bfloat16 [64, 1024, 2048], P(('grp', 'fs'), None, 'tp'), parts along dimension 0
- mixture: bfloat16 [24576, 2048], P(('grp', 'fs'), 'tp'), parts along dimension 0
There are 2 independent parts, one for each index of `grp`. A program takes and returns all parts, laid end to end along the dimension named above; an argument that names none is the same for every part. Nothing has to cross between parts.
Inputs may be any that keep to these rules, and one draw needn't show every extreme that they name: `routes`: each row names two different experts of one group (expert e lies in group e // 8). In each aligned block of 384 rows no expert is named more than 36 times, and every expert of one group is named exactly 36 times.
All inputs are finite; a program needn't handle non-finite values.
Results may differ from a plain program's by a relative error of at most 0.0087.
Values may be sent and summed in bfloat16 or wider, within the bound.
No kernel may reach another device: no remote copies, remote signals or barrier semaphores. Data moves between devices by JAX's collectives and lax.ppermute only.
A program may use at most 64 MiB of HBM per device.

v0:
```python
import jax
import jax.numpy as jnp
from jax import lax
from jax.sharding import Mesh
from jax.sharding import PartitionSpec as P

CAP = 36
FS = ("fs_0", "fs_1")
GRP_FS = ("grp", "fs_0", "fs_1")
epsilon = 1e-06


def in_blocks(x, dim, length):
    before, after = (x.shape[:dim], x.shape[dim + 1 :])
    return jnp.moveaxis(x.reshape(*before, length, -1, *after), dim, 0)


def laid_out(blocks, dim):
    blocks = jnp.moveaxis(blocks, 0, dim)
    shape = blocks.shape
    return blocks.reshape(*shape[:dim], shape[dim] * shape[dim + 1], *shape[dim + 2 :])


def exchange_in_order(blocks, axes, order):
    shape = [lax.axis_size(a) for a in axes]
    blocks = blocks.reshape(*shape, *blocks.shape[1:])
    for k in order:
        blocks = lax.all_to_all(blocks, axes[k], split_axis=k, concat_axis=k, tiled=True)
    return blocks.reshape(-1, *blocks.shape[len(axes) :])


def exchange_by_chip(x, groups, order, split_dim, concat_dim):
    length = lax.axis_size(groups[0]) * lax.axis_size(groups[1])
    blocks = in_blocks(x, split_dim, length)
    return laid_out(exchange_in_order(blocks, groups, order), concat_dim)


def normalize(rows):
    values = rows.astype(jnp.float32)
    scale = lax.rsqrt(jnp.mean(values * values, axis=-1, keepdims=True) + epsilon)
    return (values * scale).astype(jnp.bfloat16)


def shards(tokens, norm_gain, gate_weight, up_weight, down_weight, routes, route_weights):
    experts = gate_weight.shape[0]
    n_shards = lax.axis_size(FS)
    local_experts = experts // n_shards
    tok_rows = tokens.shape[0]
    gate_low = (norm_gain[None, :, None] * gate_weight).astype(jnp.bfloat16)
    up_low = (norm_gain[None, :, None] * up_weight).astype(jnp.bfloat16)
    down_low = down_weight.astype(jnp.bfloat16)
    gate_serve, up_serve = (
        lax.all_to_all(gate_low, FS, split_axis=0, concat_axis=1, tiled=True),
        lax.all_to_all(up_low, FS, split_axis=0, concat_axis=1, tiled=True),
    )
    flat_routes = routes.reshape(-1)
    expert_ids = lax.iota(jnp.int32, experts)
    onehot = (flat_routes[:, None] == expert_ids[None, :]).astype(jnp.int32)
    position = jnp.sum((jnp.cumsum(onehot, axis=0) - 1) * onehot, axis=1)
    slot_index = (flat_routes * CAP + position).reshape(tok_rows, 2)
    slot_ids = lax.iota(jnp.int32, experts * CAP)
    select = jnp.any(slot_ids[:, None, None] == slot_index[None, :, :], axis=2).astype(jnp.bfloat16)
    outbound = jnp.dot(select, tokens, preferred_element_type=jnp.float32).astype(jnp.bfloat16)
    outbound = outbound.reshape(n_shards, local_experts, CAP, outbound.shape[1])
    arrived = lax.all_to_all(outbound, FS, split_axis=0, concat_axis=2, tiled=True)[0]
    expert_rows = normalize(lax.all_gather(arrived, "tp", axis=2, tiled=True))
    gate_part = jnp.einsum(
        "erd,edh->erh", expert_rows, gate_serve, preferred_element_type=jnp.float32
    )
    up_part = jnp.einsum("erd,edh->erh", expert_rows, up_serve, preferred_element_type=jnp.float32)
    hidden = (jax.nn.silu(gate_part) * up_part).astype(jnp.bfloat16)
    down_serve = lax.all_to_all(down_low, FS, split_axis=0, concat_axis=1, tiled=True)
    expert_out = jnp.einsum(
        "erk,ekd->erd",
        lax.all_gather(hidden, "tp", axis=2, tiled=True),
        down_serve,
        preferred_element_type=jnp.float32,
    ).astype(jnp.bfloat16)
    expert_out = expert_out.reshape(1, local_experts, hidden.shape[1], expert_out.shape[2])
    returned_rows = exchange_by_chip(expert_out, ("fs_0", "fs_1"), (1, 0), 2, 0)
    returned_rows = returned_rows.reshape(experts * CAP, returned_rows.shape[3])
    picked = returned_rows[slot_index]
    mixture = jnp.sum(route_weights[:, :, None] * picked.astype(jnp.float32), axis=1).astype(
        jnp.bfloat16
    )
    return (gate_serve, up_serve, down_serve, mixture)


def solution(mesh):
    split = Mesh(
        mesh.devices.reshape(mesh.shape["grp"], 16, 2, mesh.shape["tp"]),
        ("grp", "fs_0", "fs_1", "tp"),
    )
    placed = (
        P(GRP_FS, "tp"),
        P(FS),
        P(None, FS, "tp"),
        P(None, FS, "tp"),
        P(None, FS, "tp"),
        P(GRP_FS, None),
        P(GRP_FS, None),
    )
    return jax.shard_map(
        shards,
        mesh=split,
        in_specs=placed,
        out_specs=(
            P(GRP_FS, None, "tp"),
            P(GRP_FS, None, "tp"),
            P(GRP_FS, None, "tp"),
            P(GRP_FS, "tp"),
        ),
        check_vma=False,
    )
```

profile of v0, /device:TPU:66, one launch (start us, length us, event | category | flops | bytes accessed | tf_op | source)
XLA Modules:
  0.0 293.5 jit_solution(14518242084303444602)
XLA Ops:
  7.2 0.1 all-gather.4.cloned.1.call-start
  7.3 0.9 copy.41
  8.2 0.1 eq.43
  8.3 0.1 eq.39
  8.5 1.7 reduce-window.6
  10.3 0.3 slice_reduce_fusion
  10.5 0.1 fusion.9
  10.7 0.2 reduce_sum.30
  10.8 0.1 copy.44
  10.9 0.7 compare_select_fusion
  11.6 0.8 fusion.3
  12.4 0.5 convolution_convert_fusion.1
  12.9 0.1 reshape.99
  13.0 82.9 %all_to_all.55 = bf16[32,1,36,256]{3,2,1,0:T(8,128)(2,1)S(1)} all-to-all(bf16[32,1,36,256]{3,2,1,0:T(8,128)(2,1)S(1)} %bitcast.35), channel_id=1, replica_groups=mesh['grp'=2,'fs_0'=16,'fs_1'=2,'tp'=8] {'fs_0','fs_1'}, dimensions={0} | all-to-all | bytes 1179648 | tf_op jit(solution)/shard_map/all_to_all | solution.py:65
  95.9 0.9 squeeze.3
  96.9 0.1 all-gather.4.cloned.1.call-update
  96.9 2.3 multiply_convert_fusion
  99.2 37.1 %all_to_all.56 = bf16[32,64,128]{2,1,0:T(8,128)(2,1)S(1)} all-to-all(bf16[32,64,128]{2,1,0:T(8,128)(2,1)S(1)} %get-tuple-element.7), channel_id=1, replica_groups=mesh['grp'=2,'fs_0'=16,'fs_1'=2,'tp'=8] {'fs_0','fs_1'}, dimensions={0} | all-to-all | bytes 1048576 | tf_op jit(solution)/shard_map/all_to_all | solution.py:53
  136.3 4.8 %all-to-all-start.1 = ((bf16[32,64,128]{2,1,0:T(8,128)(2,1)}), bf16[32,64,128]{2,1,0:T(8,128)(2,1)S(1)}, u32[]{:S(2)}, u32[]{:S(2)}) async-start(bf16[32,64,128]{2,1,0:T(8,128)(2,1)} %get-tuple-element.6), calls=%async_computation.1 | async-start | bytes 1048576 | tf_op jit(solution)/shard_map/all_to_all | solution.py:54
  141.1 0.1 all-gather.6.cloned.1.call-start
  141.2 22.0 %all-gather.4.cloned.1.call-done = bf16[1,1152,2048]{2,1,0:T(8,128)(2,1)} async-done(((bf16[1,1152,256]{2,1,0:T(8,128)(2,1)}), bf16[1,1152,2048]{2,1,0:T(8,128)(2,1)}) %all-gather.4.cloned.1.call-update) | async-done | bytes 4718608 | tf_op jit(solution)/shard_map/all_gather | solution.py:66
  163.2 3.5 %fusion = f32[1152]{0:T(1024)S(1)} fusion(bf16[1,1152,2048]{2,1,0:T(8,128)(2,1)} %all-gather.4.cloned.1.call-done), kind=kLoop, calls=%fused_computation.3 | loop fusion | flops 7076736 | bytes 4723200 | tf_op jit(solution)/shard_map/reduce_sum | solution.py:40
  166.7 0.3 copy-done.1
  167.0 1.5 fusion.6
  168.5 5.8 %all-to-all-done.1 = bf16[32,64,128]{2,1,0:T(8,128)(2,1)S(1)} async-done(((bf16[32,64,128]{2,1,0:T(8,128)(2,1)}), bf16[32,64,128]{2,1,0:T(8,128)(2,1)S(1)}, u32[]{:S(2)}, u32[]{:S(2)}) %all-to-all-start.1) | async-done | bytes 524320 | tf_op jit(solution)/shard_map/all_to_all | solution.py:54
  174.3 4.6 %fusion.4 = bf16[1152,128]{1,0:T(8,128)(2,1)} fusion(bf16[2048,128]{1,0:T(8,128)(2,1)S(1)} %bitcast.38, bf16[1,1152,2048]{2,1,0:T(8,128)(2,1)} %all-gather.4.cloned.1.call-done, f32[1152]{0:T(1024)S(1)} %add_rsqrt_fusion, f32[1152,128]{1,0:T(8,128)S(1)} %fusion.6), kind=kOutput, calls=%fused_computation.11 | convolution fusion | flops 611942400 | bytes 6132224 | tf_op jit(solution)/shard_map/erd,edh->erh/dot_general | solution.py:70
  178.9 0.1 all-gather.6.cloned.1.call-update
  179.0 0.1 convert_element_type.42
  179.0 38.7 %all_to_all.57 = bf16[32,32,256]{2,1,0:T(8,128)(2,1)S(1)} all-to-all(bf16[32,32,256]{2,1,0:T(8,128)(2,1)S(1)} %convert_element_type.42), channel_id=1, replica_groups=mesh['grp'=2,'fs_0'=16,'fs_1'=2,'tp'=8] {'fs_0','fs_1'}, dimensions={0} | all-to-all | bytes 1048576 | tf_op jit(solution)/shard_map/all_to_all | solution.py:72
  217.8 9.2 %all-gather.6.cloned.1.call-done = bf16[1152,1024]{1,0:T(8,128)(2,1)} async-done(((bf16[1152,128]{1,0:T(8,128)(2,1)}), bf16[1152,1024]{1,0:T(8,128)(2,1)}) %all-gather.6.cloned.1.call-update) | async-done | bytes 2359312 | tf_op jit(solution)/shard_map/all_gather | solution.py:75
  226.9 2.4 convolution_convert_fusion
  229.4 0.1 reshape_transpose_reshape_reshape.3
  229.5 0.2 copy.46
  229.7 4.2 %all_to_all.58 = bf16[16,2,1,1,36,256]{5,0,4,3,2,1:T(8,128)(2,1)S(1)} all-to-all(bf16[16,2,1,1,36,256]{5,0,4,3,2,1:T(8,128)(2,1)S(1)} %copy.46), channel_id=1, replica_groups=mesh['grp'=2,'fs_0'=16,'fs_1'=2,'tp'=8] {'fs_1'}, dimensions={1} | all-to-all | bytes 1179648 | tf_op jit(solution)/shard_map/all_to_all | solution.py:28
  233.9 1.4 copy.47
  235.3 13.1 %all-to-all-start.5 = ((bf16[16,2,1,1,36,256]{5,1,4,3,2,0:T(2,128)(2,1)}), bf16[16,2,1,1,36,256]{5,1,4,3,2,0:T(2,128)(2,1)S(1)}, u32[]{:S(2)}, u32[]{:S(2)}) async-start(bf16[16,2,1,1,36,256]{5,1,4,3,2,0:T(2,128)(2,1)} %copy.47), calls=%async_computation.5 | async-start | bytes 1179648 | tf_op jit(solution)/shard_map/all_to_all | solution.py:28
  248.4 0.1 copy.49
  248.6 0.1 reshape.107
  248.7 0.1 copy.40
  248.9 30.4 %all-to-all-done.5 = bf16[16,2,1,1,36,256]{5,1,4,3,2,0:T(2,128)(2,1)S(1)} async-done(((bf16[16,2,1,1,36,256]{5,1,4,3,2,0:T(2,128)(2,1)}), bf16[16,2,1,1,36,256]{5,1,4,3,2,0:T(2,128)(2,1)S(1)}, u32[]{:S(2)}, u32[]{:S(2)}) %all-to-all-start.5) | async-done | bytes 589856 | tf_op jit(solution)/shard_map/all_to_all | solution.py:28
  279.3 0.1 copy.48
  279.3 0.1 reshape_reshape_reshape.3
  279.5 2.7 gather_fusion
  282.1 0.4 reshape.117
  282.5 1.7 multiply_reduce_fusion
  284.2 0.8 copy.55
  285.0 0.8 copy.56
  285.8 0.8 copy.57
  (15 shorter events, 0.1 us)
Async XLA Ops:
  7.2 5.2 %copy-start = (bf16[384,256]{1,0:T(8,128)(2,1)S(1)}, bf16[384,256]{1,0:T(8,128)(2,1)}, u32[]{:S(2)}) copy-start(bf16[384,256]{1,0:T(8,128)(2,1)} %param.7) | copy-start | bytes 589828
  7.2 89.7 %copy-start.3 = (f32[32,64,128]{2,1,0:T(8,128)S(1)}, f32[32,64,128]{2,1,0:T(8,128)}, u32[]{:S(2)}) copy-start(f32[32,64,128]{2,1,0:T(8,128)} %param.10) | copy-start | bytes 3145732
  7.2 89.7 %copy-start.5 = (f32[64]{0:T(128)S(1)}, f32[64]{0:T(128)}, u32[]{:S(2)}) copy-start(f32[64]{0:T(128)} %param.8) | copy-start | bytes 772
  7.2 156.0 %all-gather.4.cloned.1.call-start = ((), (), s32[]{:S(2)}) async-start(), calls=%async_computation.6 | async-start | bytes 5308416 | tf_op jit(solution)/shard_map/all_gather | solution.py:66
  136.3 38.0 %all-to-all-start.1 = ((bf16[32,64,128]{2,1,0:T(8,128)(2,1)}), bf16[32,64,128]{2,1,0:T(8,128)(2,1)S(1)}, u32[]{:S(2)}, u32[]{:S(2)}) async-start(bf16[32,64,128]{2,1,0:T(8,128)(2,1)} %get-tuple-element.6), calls=%async_computation.1 | async-start | bytes 1048576 | tf_op jit(solution)/shard_map/all_to_all | solution.py:54
  141.1 85.8 %all-gather.6.cloned.1.call-start = ((), (), s32[]{:S(2)}) async-start(), calls=%async_computation.7 | async-start | bytes 2654208 | tf_op jit(solution)/shard_map/all_gather | solution.py:75
  163.2 3.8 %copy-start.1 = (bf16[1,1152,2048]{2,1,0:T(8,128)(2,1)S(1)}, bf16[1,1152,2048]{2,1,0:T(8,128)(2,1)}, u32[]{:S(2)}) copy-start(bf16[1,1152,2048]{2,1,0:T(8,128)(2,1)} %all-gather.4.cloned.1.call-done) | copy-start | bytes 14155780
  174.3 4.7 %copy-start.2 = (f32[32,32,256]{2,1,0:T(8,128)S(1)}, f32[32,32,256]{2,1,0:T(8,128)}, u32[]{:S(2)}) copy-start(f32[32,32,256]{2,1,0:T(8,128)} %param.11) | copy-start | bytes 3145732
  229.4 19.4 %copy-start.4 = (f32[384,2]{0,1:T(2,128)S(1)}, f32[384,2]{0,1:T(2,128)}, u32[]{:S(2)}) copy-start(f32[384,2]{0,1:T(2,128)} %param.13) | copy-start | bytes 9220
  235.3 43.9 %all-to-all-start.5 = ((bf16[16,2,1,1,36,256]{5,1,4,3,2,0:T(2,128)(2,1)}), bf16[16,2,1,1,36,256]{5,1,4,3,2,0:T(2,128)(2,1)S(1)}, u32[]{:S(2)}, u32[]{:S(2)}) async-start(bf16[16,2,1,1,36,256]{5,1,4,3,2,0:T(2,128)(2,1)} %copy.47), calls=%async_computation.5 | async-start | bytes 1179648 | tf_op jit(solution)/shard_map/all_to_all | solution.py:28
Sparse Core Ops, SparseCore 0:
  97.0 66.1 all-gather.3
  179.1 47.8 all-gather.5
where the time goes:
time: 294 us; the launch traced here: 293 us
  blocking collectives  163 us (55%)
  waiting for transfers between devices  67.5 us (23%)
  starting transfers between devices  18 us (6%)
  between operations  14.3 us (5%)
  other arithmetic  10.9 us (4%)
  local copies, waits for them, and re-layouts  10.8 us (4%)
  matrix products  8.96 us (3%)
    all_to_all x1, blocking collectives, shards(): lax.all_to_all(outbound, FS, split_axis=0, concat_axis=2, tiled=True)[0]  82.9 us
    all_to_all x1, blocking collectives, shards(): lax.all_to_all(down_low, FS, split_axis=0, concat_axis=1, tiled=True)  38.7 us
    all_to_all x1, blocking collectives, shards(): lax.all_to_all(gate_low, FS, split_axis=0, concat_axis=1, tiled=True)  37.1 us
    all_to_all x1, waiting for transfers between devices, exchange_in_order(): lax.all_to_all(blocks, axes[k], split_axis=k, concat_axis=k, tiled=True)  30.4 us
    all_gather x1, waiting for transfers between devices, shards(): expert_rows = normalize(lax.all_gather(arrived, 'tp', axis=2, tiled=True))  22 us
    all_to_all x1, starting transfers between devices, exchange_in_order(): lax.all_to_all(blocks, axes[k], split_axis=k, concat_axis=k, tiled=True)  13.1 us
    all_gather x1, waiting for transfers between devices, shards(): lax.all_gather(hidden, 'tp', axis=2, tiled=True)  9.16 us
  transfers between devices with their start and end apart: 4, of which 4 were waited for; matrix products, arithmetic and copies ran while one was open for 3% of the time, Pallas kernels for 0%

commit v1 on v0

--- a/solution.py
+++ b/solution.py
@@ -1,3 +1,4 @@
+import functools
 import jax
 import jax.numpy as jnp
 from jax import lax
@@ -8,6 +9,16 @@
 FS = ("fs_0", "fs_1")
 GRP_FS = ("grp", "fs_0", "fs_1")
 epsilon = 1e-06
+
+
+def turn_core_for(vals, dim_i):
+    return jnp.concatenate(
+        lax.all_to_all(jnp.stack(tuple((vals for _ in range(lax.psum(1, "tp"))))), "tp", 0, 0),
+        axis=dim_i,
+    )
+
+
+stocks_produce = functools.partial(turn_core_for, dim_i=2)
 
 
 def in_blocks(x, dim, length):
@@ -63,7 +74,7 @@
     outbound = jnp.dot(select, tokens, preferred_element_type=jnp.float32).astype(jnp.bfloat16)
     outbound = outbound.reshape(n_shards, local_experts, CAP, outbound.shape[1])
     arrived = lax.all_to_all(outbound, FS, split_axis=0, concat_axis=2, tiled=True)[0]
-    expert_rows = normalize(lax.all_gather(arrived, "tp", axis=2, tiled=True))
+    expert_rows = normalize(stocks_produce(arrived))
     gate_part = jnp.einsum(
         "erd,edh->erh", expert_rows, gate_serve, preferred_element_type=jnp.float32
     )

time: 294 us -> 404 us (1.37)
  waiting for transfers between devices: 67.5 us -> 130 us
  starting transfers between devices: 18 us -> 67.5 us
  blocking collectives: 163 us -> 155 us
  local copies, waits for them, and re-layouts: 10.8 us -> 15.4 us
    all_to_all x0 -> x2, waiting for transfers between devices: none -> 70.1 us  [the longest x1 37.4 us: shards(): lax.all_to_all(outbound, FS, split_axis=0, concat_axis=2, tiled=True)[0]]
    all_to_all x0 -> x2, starting transfers between devices: none -> 49.3 us  [the longest x1 44.4 us: shards(): lax.all_to_all(outbound, FS, split_axis=0, concat_axis=2, tiled=True)[0]]
    all_gather x1 -> x0, waiting for transfers between devices: 22 us -> none  [shards(): expert_rows = normalize(lax.all_gather(arrived, 'tp', axis=2, tiled=True))]
    all_to_all x1, waiting for transfers between devices: 5.82 us -> 23.6 us  [shards(): lax.all_to_all(up_low, FS, split_axis=0, concat_axis=1, tiled=True)]
    all_to_all x2 -> x1, blocking collectives: 120 us -> 113 us  [turn_core_for(): lax.all_to_all(jnp.stack(tuple((vals for _ in range(lax.psum(1, 'tp')))))...]
  transfers between devices with their start and end apart: 4 -> 5, of which waited for: 4 -> 5; matrix products, arithmetic and copies ran while one was open for 3% -> 2% of each run, Pallas kernels for 0% -> 0%
where the time goes in v1:
time: 404 us; the launch traced here: 403 us
  blocking collectives  155 us (38%)
  waiting for transfers between devices  130 us (32%)
  starting transfers between devices  67.5 us (17%)
  local copies, waits for them, and re-layouts  15.4 us (4%)
  between operations  14.4 us (4%)
  other arithmetic  10.6 us (3%)
  matrix products  10.3 us (3%)
    all_to_all x1, blocking collectives, turn_core_for(): lax.all_to_all(jnp.stack(tuple((vals for _ in range(lax.psum(1, 'tp')))))...  113 us
    all_to_all x1, starting transfers between devices, shards(): lax.all_to_all(outbound, FS, split_axis=0, concat_axis=2, tiled=True)[0]  44.4 us
    all_to_all x1, waiting for transfers between devices, shards(): lax.all_to_all(outbound, FS, split_axis=0, concat_axis=2, tiled=True)[0]  37.4 us
    all_to_all x1, blocking collectives, shards(): lax.all_to_all(down_low, FS, split_axis=0, concat_axis=1, tiled=True)  37.3 us
    all_to_all x1, waiting for transfers between devices, shards(): lax.all_to_all(gate_low, FS, split_axis=0, concat_axis=1, tiled=True)  32.8 us
    all_to_all x1, waiting for transfers between devices, exchange_in_order(): lax.all_to_all(blocks, axes[k], split_axis=k, concat_axis=k, tiled=True)  30.3 us
    all_to_all x1, waiting for transfers between devices, shards(): lax.all_to_all(up_low, FS, split_axis=0, concat_axis=1, tiled=True)  23.6 us
    all_to_all x1, starting transfers between devices, exchange_in_order(): lax.all_to_all(blocks, axes[k], split_axis=k, concat_axis=k, tiled=True)  13.4 us
  transfers between devices with their start and end apart: 5, of which 5 were waited for; matrix products, arithmetic and copies ran while one was open for 2% of the time, Pallas kernels for 0%

profile of v1, /device:TPU:66, one launch (start us, length us, event | category | flops | bytes accessed | tf_op | source)
XLA Modules:
  0.0 403.3 jit_solution(10945942297219220695)
XLA Ops:
  7.2 1.0 copy.49
  8.2 0.1 eq.43
  8.3 0.1 eq.39
  8.5 1.7 reduce-window.6
  10.3 0.3 slice_reduce_fusion
  10.5 0.1 fusion.7
  10.7 0.2 reduce_sum.30
  10.9 0.7 compare_select_fusion
  11.6 0.8 fusion.1
  12.4 0.5 convolution_convert_fusion.1
  12.9 1.0 reshape.167
  13.8 44.4 %all-to-all-start.3 = ((bf16[32,1,36,256]{3,2,1,0:T(8,128)(2,1)}), bf16[32,1,36,256]{3,2,1,0:T(8,128)(2,1)S(1)}, u32[]{:S(2)}, u32[]{:S(2)}) async-start(bf16[32,1,36,256]{3,2,1,0:T(8,128)(2,1)} %bitcast.4), calls=%async_computation.3 | async-start | bytes 1310720 | tf_op jit(solution)/shard_map/all_to_all | solution.py:76
  58.3 1.3 multiply_convert_fusion.1
  59.6 37.4 %all-to-all-done.3 = bf16[32,1,36,256]{3,2,1,0:T(8,128)(2,1)S(1)} async-done(((bf16[32,1,36,256]{3,2,1,0:T(8,128)(2,1)}), bf16[32,1,36,256]{3,2,1,0:T(8,128)(2,1)S(1)}, u32[]{:S(2)}, u32[]{:S(2)}) %all-to-all-start.3) | async-done | bytes 589856 | tf_op jit(solution)/shard_map/all_to_all | solution.py:76
  97.0 4.8 %all-to-all-start = ((bf16[32,64,128]{2,1,0:T(8,128)(2,1)}), bf16[32,64,128]{2,1,0:T(8,128)(2,1)S(1)}, u32[]{:S(2)}, u32[]{:S(2)}) async-start(bf16[32,64,128]{2,1,0:T(8,128)(2,1)} %get-tuple-element.7), calls=%async_computation | async-start | bytes 1048576 | tf_op jit(solution)/shard_map/all_to_all | solution.py:64
  101.8 0.1 all_to_all.52
  101.9 0.3 copy.54
  102.2 32.8 %all-to-all-done = bf16[32,64,128]{2,1,0:T(8,128)(2,1)S(1)} async-done(((bf16[32,64,128]{2,1,0:T(8,128)(2,1)}), bf16[32,64,128]{2,1,0:T(8,128)(2,1)S(1)}, u32[]{:S(2)}, u32[]{:S(2)}) %all-to-all-start) | async-done | bytes 524320 | tf_op jit(solution)/shard_map/all_to_all | solution.py:64
  135.0 0.6 stack.3
  135.6 113.4 %all_to_all.63 = bf16[8,1,1152,256]{2,3,1,0:T(8,128)(2,1)} all-to-all(bf16[8,1,1152,256]{2,3,1,0:T(8,128)(2,1)S(1)} %stack.3), channel_id=1, replica_groups=mesh['grp'=2,'fs_0'=16,'fs_1'=2,'tp'=8] {'tp'}, dimensions={0} | all-to-all | bytes 9437184 | tf_op jit(solution)/shard_map/all_to_all | solution.py:16
  249.0 4.8 %all-to-all-start.1 = ((bf16[32,64,128]{2,1,0:T(8,128)(2,1)}), bf16[32,64,128]{2,1,0:T(8,128)(2,1)S(1)}, u32[]{:S(2)}, u32[]{:S(2)}) async-start(bf16[32,64,128]{2,1,0:T(8,128)(2,1)} %get-tuple-element.6), calls=%async_computation.1 | async-start | bytes 1048576 | tf_op jit(solution)/shard_map/all_to_all | solution.py:65
  253.9 3.5 multiply_reduce_fusion
  257.4 0.3 copy-done.2
  257.6 0.6 bitcast_convert_fusion
  258.3 3.6 copy-done.1
  261.9 1.4 fusion.4
  263.3 23.6 %all-to-all-done.1 = bf16[32,64,128]{2,1,0:T(8,128)(2,1)S(1)} async-done(((bf16[32,64,128]{2,1,0:T(8,128)(2,1)}), bf16[32,64,128]{2,1,0:T(8,128)(2,1)S(1)}, u32[]{:S(2)}, u32[]{:S(2)}) %all-to-all-start.1) | async-done | bytes 524320 | tf_op jit(solution)/shard_map/all_to_all | solution.py:65
  287.0 5.9 %fusion.2 = bf16[1152,128]{1,0:T(8,128)(2,1)} fusion(bf16[2048,128]{1,0:T(8,128)(2,1)S(1)} %bitcast.46, f32[1,1152,1,1,1,1,2048]{1,6,5,4,3,2,0:T(8,128)} %bitcast.45, f32[1152]{0:T(1024)S(1)} %add_rsqrt_fusion, f32[1152,128]{1,0:T(8,128)S(1)} %fusion.4), kind=kOutput, calls=%fused_computation.10 | convolution fusion | flops 609583104 | bytes 10850816 | tf_op jit(solution)/shard_map/erd,edh->erh/dot_general | solution.py:81
  293.1 37.3 %all_to_all.64 = bf16[32,32,256]{2,1,0:T(8,128)(2,1)S(1)} all-to-all(bf16[32,32,256]{2,1,0:T(8,128)(2,1)S(1)} %convert_element_type.97), channel_id=1, replica_groups=mesh['grp'=2,'fs_0'=16,'fs_1'=2,'tp'=8] {'fs_0','fs_1'}, dimensions={0} | all-to-all | bytes 1048576 | tf_op jit(solution)/shard_map/all_to_all | solution.py:83
  330.3 6.2 %all-gather.3.cloned.1.call-done = bf16[1152,1024]{1,0:T(8,128)(2,1)} async-done(((bf16[1152,128]{1,0:T(8,128)(2,1)}), bf16[1152,1024]{1,0:T(8,128)(2,1)}) %all-gather.3.cloned.1.call-update) | async-done | bytes 2359312 | tf_op jit(solution)/shard_map/all_gather | solution.py:86
  336.5 2.4 convolution_convert_fusion
  338.9 0.1 reshape_transpose_reshape_reshape.3
  339.0 0.2 copy.57
  339.2 4.2 %all_to_all.65 = bf16[16,2,1,1,36,256]{5,0,4,3,2,1:T(8,128)(2,1)S(1)} all-to-all(bf16[16,2,1,1,36,256]{5,0,4,3,2,1:T(8,128)(2,1)S(1)} %copy.57), channel_id=1, replica_groups=mesh['grp'=2,'fs_0'=16,'fs_1'=2,'tp'=8] {'fs_1'}, dimensions={1} | all-to-all | bytes 1179648 | tf_op jit(solution)/shard_map/all_to_all | solution.py:39
  343.5 1.4 copy.58
  344.9 13.4 %all-to-all-start.6 = ((bf16[16,2,1,1,36,256]{5,1,4,3,2,0:T(2,128)(2,1)}), bf16[16,2,1,1,36,256]{5,1,4,3,2,0:T(2,128)(2,1)S(1)}, u32[]{:S(2)}, u32[]{:S(2)}) async-start(bf16[16,2,1,1,36,256]{5,1,4,3,2,0:T(2,128)(2,1)} %copy.58), calls=%async_computation.6 | async-start | bytes 1179648 | tf_op jit(solution)/shard_map/all_to_all | solution.py:39
  358.3 0.1 copy.60
  358.4 0.1 reshape.175
  358.6 0.1 copy.48
  358.7 30.3 %all-to-all-done.6 = bf16[16,2,1,1,36,256]{5,1,4,3,2,0:T(2,128)(2,1)S(1)} async-done(((bf16[16,2,1,1,36,256]{5,1,4,3,2,0:T(2,128)(2,1)}), bf16[16,2,1,1,36,256]{5,1,4,3,2,0:T(2,128)(2,1)S(1)}, u32[]{:S(2)}, u32[]{:S(2)}) %all-to-all-start.6) | async-done | bytes 589856 | tf_op jit(solution)/shard_map/all_to_all | solution.py:39
  389.1 0.1 copy.59
  389.1 0.1 reshape_reshape_reshape.3
  389.3 2.7 gather_fusion
  391.9 0.4 reshape.185
  392.3 1.7 multiply_reduce_fusion.1
  394.0 0.8 copy.66
  394.8 0.8 copy.67
  395.6 0.8 copy.68
  (22 shorter events, 0.4 us)
Async XLA Ops:
  7.2 5.2 %copy-start = (bf16[384,256]{1,0:T(8,128)(2,1)S(1)}, bf16[384,256]{1,0:T(8,128)(2,1)}, u32[]{:S(2)}) copy-start(bf16[384,256]{1,0:T(8,128)(2,1)} %param.7) | copy-start | bytes 589828
  7.2 51.1 %copy-start.4 = (f32[32,64,128]{2,1,0:T(8,128)S(1)}, f32[32,64,128]{2,1,0:T(8,128)}, u32[]{:S(2)}) copy-start(f32[32,64,128]{2,1,0:T(8,128)} %param.10) | copy-start | bytes 3145732
  7.2 51.1 %copy-start.7 = (f32[64]{0:T(128)S(1)}, f32[64]{0:T(128)}, u32[]{:S(2)}) copy-start(f32[64]{0:T(128)} %param.8) | copy-start | bytes 772
  7.2 51.1 %copy-start.5 = (f32[32,64,128]{2,1,0:T(8,128)S(1)}, f32[32,64,128]{2,1,0:T(8,128)}, u32[]{:S(2)}) copy-start(f32[32,64,128]{2,1,0:T(8,128)} %param.9) | copy-start | bytes 3145732
  13.8 83.1 %all-to-all-start.3 = ((bf16[32,1,36,256]{3,2,1,0:T(8,128)(2,1)}), bf16[32,1,36,256]{3,2,1,0:T(8,128)(2,1)S(1)}, u32[]{:S(2)}, u32[]{:S(2)}) async-start(bf16[32,1,36,256]{3,2,1,0:T(8,128)(2,1)} %bitcast.4), calls=%async_computation.3 | async-start | bytes 1310720 | tf_op jit(solution)/shard_map/all_to_all | solution.py:76
  97.0 38.0 %all-to-all-start = ((bf16[32,64,128]{2,1,0:T(8,128)(2,1)}), bf16[32,64,128]{2,1,0:T(8,128)(2,1)S(1)}, u32[]{:S(2)}, u32[]{:S(2)}) async-start(bf16[32,64,128]{2,1,0:T(8,128)(2,1)} %get-tuple-element.7), calls=%async_computation | async-start | bytes 1048576 | tf_op jit(solution)/shard_map/all_to_all | solution.py:64
  249.0 38.0 %all-to-all-start.1 = ((bf16[32,64,128]{2,1,0:T(8,128)(2,1)}), bf16[32,64,128]{2,1,0:T(8,128)(2,1)S(1)}, u32[]{:S(2)}, u32[]{:S(2)}) async-start(bf16[32,64,128]{2,1,0:T(8,128)(2,1)} %get-tuple-element.6), calls=%async_computation.1 | async-start | bytes 1048576 | tf_op jit(solution)/shard_map/all_to_all | solution.py:65
  253.8 82.7 %all-gather.3.cloned.1.call-start = ((), (), s32[]{:S(2)}) async-start(), calls=%async_computation.7 | async-start | bytes 2654208 | tf_op jit(solution)/shard_map/all_gather | solution.py:86
  253.9 3.8 copy-start.2
  258.3 3.6 copy-start.1
  287.0 6.0 %copy-start.3 = (f32[32,32,256]{2,1,0:T(8,128)S(1)}, f32[32,32,256]{2,1,0:T(8,128)}, u32[]{:S(2)}) copy-start(f32[32,32,256]{2,1,0:T(8,128)} %param.11) | copy-start | bytes 3145732
  338.9 19.6 %copy-start.6 = (f32[384,2]{0,1:T(2,128)S(1)}, f32[384,2]{0,1:T(2,128)}, u32[]{:S(2)}) copy-start(f32[384,2]{0,1:T(2,128)} %param.13) | copy-start | bytes 9220
  344.9 44.2 %all-to-all-start.6 = ((bf16[16,2,1,1,36,256]{5,1,4,3,2,0:T(2,128)(2,1)}), bf16[16,2,1,1,36,256]{5,1,4,3,2,0:T(2,128)(2,1)S(1)}, u32[]{:S(2)}, u32[]{:S(2)}) async-start(bf16[16,2,1,1,36,256]{5,1,4,3,2,0:T(2,128)(2,1)} %copy.58), calls=%async_computation.6 | async-start | bytes 1179648 | tf_op jit(solution)/shard_map/all_to_all | solution.py:39
Sparse Core Ops, SparseCore 0:
  293.1 43.3 all-gather.2
